TPU v7x, 32 devices: a whole 2x2x4 slice. The times are simulated.
32 devices in a mesh: sp: 4 (over y, x), tp: 8 (over z, core).
Axes of the slice: x: 2, y: 2, z: 4, core: 2. Of those that a mesh axis runs over, the one named last changes fastest.
Arguments:
- cotangent: bfloat16 [1024, 2048], P('sp', 'tp'), may hold values from -6 to 6
- block_input: bfloat16 [1024, 2048], P('sp', 'tp'), may hold values from -6 to 6
- routes: int32 [1024, 2], P('sp'), may hold values from 0 to 3, all different within a row; in each aligned block of 256 rows (0 to 255, 256 to 511, ...) at most 160 rows name the same one
- route_weights: float32 [1024, 2], P('sp'), may hold values from 0.1 to 0.9
- gate_weight: bfloat16 [4, 2048, 7168], P('sp', None, 'tp'), may hold values from -0.125 to 0.125
- up_weight: bfloat16 [4, 2048, 7168], P('sp', None, 'tp'), may hold values from -0.125 to 0.125
- down_weight: bfloat16 [4, 7168, 2048], P('sp', 'tp'), may hold values from -0.0625 to 0.0625
- out_weight: bfloat16 [1024, 2048], P('tp'), may hold values from -0.1875 to 0.1875
- conv_out: bfloat16 [1024, 1024], P('tp', 'sp'), may hold values from -6 to 6
- gate_pre: bfloat16 [1024, 1024], P('tp', 'sp'), may hold values from -6 to 6
- prior_states: bfloat16 [1024, 1024], P('tp', 'sp'), may hold values from -6 to 6
- recur_weight: bfloat16 [16, 64, 64], replicated, may hold values from -0.75 to 0.75
- input_gate_matrix: bfloat16 [16, 64, 64], replicated, may hold values from -0.75 to 0.75
- decay_param: float32 [1024], replicated, may hold values from 4 to 16
- decay_jump: float32 [1024, 1024], P('tp', 'sp'), may hold values from -1 to 0, as said below
Outputs:
- gate_weight_grad: bfloat16 [4, 2048, 7168], P('sp', None, 'tp')
- up_weight_grad: bfloat16 [4, 2048, 7168], P('sp', None, 'tp')
- down_weight_grad: bfloat16 [4, 7168, 2048], P('sp', 'tp')
- out_weight_grad: float32 [1024, 2048], P('tp', 'sp')
- conv_grad: bfloat16 [1024, 1024], P('tp', 'sp')
- valve_logit_derivative: bfloat16 [1024, 1024], P('tp', 'sp')
Inputs may be any that keep to these rules, and one draw needn't show every extreme that they name: In each aligned block of 256 rows (the rows of one index of sp) no expert is named by more than 160 routes, a bound that some block reaches; a row names 2 different experts. `decay_jump`: every entry is at most -1 / 20480.
All inputs are finite; a program needn't handle non-finite values.
Results may differ from a plain program's by a relative error of at most 0.018.
Values may be sent and summed in bfloat16 or wider, within the bound.
A program may use at most 128 MiB of HBM per device.

v0:
```python
import jax
import jax.numpy as jnp
from jax import lax
from jax.sharding import PartitionSpec as P

HEAD_DIM = 64
TOP_K = 2
RATE_SCALE = 8.0


def prefix(value, axis, join, neutral):
    count, mine = (lax.axis_size(axis), lax.axis_index(axis))
    pieces = jax.tree.map(lambda part: lax.all_gather(part, axis), value)
    pieces = jax.tree.map(lambda part: part[::-1], pieces)
    mine = count - 1 - mine
    so_far = jax.tree.map(
        lambda part, zero: jnp.full_like(part, 0) + jnp.asarray(zero, part.dtype), value, neutral
    )

    def turn(position, so_far):
        longer = join(so_far, jax.tree.map(lambda part: part[position], pieces))
        return jax.tree.map(lambda new, old: jnp.where(position < mine, new, old), longer, so_far)

    return lax.fori_loop(0, count - 1, turn, so_far)


def link_pairs(left_pair, right_pair):
    return (left_pair[0] * right_pair[0], right_pair[0] * left_pair[1] + right_pair[1])


def later_first(earlier_pair, later_pair):
    return (earlier_pair[0] * later_pair[0], later_pair[1] + later_pair[0] * earlier_pair[1])


def routing_tables(routes, experts, capacity):
    flat_routes = routes.reshape(-1)
    onehot = (flat_routes[:, None] == jnp.arange(experts, dtype=jnp.int32)[None, :]).astype(
        jnp.int32
    )
    slot_rank = jnp.sum((jnp.cumsum(onehot, axis=0) - onehot) * onehot, axis=1)
    target = (flat_routes * capacity + slot_rank).reshape(routes.shape[0], routes.shape[1])
    slot_ids = jnp.arange(experts * capacity, dtype=jnp.int32)
    return jnp.transpose(target)[:, None, :] == slot_ids[None, :, None]


def spread(placing, route_hits, rows_in, cot_in, route_weights):
    sent_rows = jnp.dot(placing, rows_in, preferred_element_type=jnp.float32).astype(jnp.bfloat16)
    scaled = (
        jnp.transpose(route_weights)[:, :, None] * cot_in.astype(jnp.float32)[None, :, :]
    ).astype(jnp.bfloat16)
    sent_cot = jnp.einsum(
        "kst,ktd->sd", route_hits, scaled, preferred_element_type=jnp.float32
    ).astype(jnp.bfloat16)
    return (sent_rows, sent_cot)


def expert_work(slot_rows, slot_cot, w_gate, w_up, w_down):
    minor = (((1,), (1,)), ((), ()))
    gate_act = jnp.dot(slot_rows, w_gate, preferred_element_type=jnp.float32)
    up_act = jnp.dot(slot_rows, w_up, preferred_element_type=jnp.float32)
    sigma_gate = jax.nn.sigmoid(gate_act)
    silu_val = gate_act * sigma_gate
    hidden = (silu_val * up_act).astype(jnp.bfloat16)
    d_hidden = lax.dot_general(slot_cot, w_down, minor, preferred_element_type=jnp.float32)
    d_gate = (d_hidden * up_act * sigma_gate * (1.0 + gate_act * (1.0 - sigma_gate))).astype(
        jnp.bfloat16
    )
    d_up = (d_hidden * silu_val).astype(jnp.bfloat16)
    width_part = lax.dot_general(d_gate, w_gate, minor, preferred_element_type=jnp.float32)
    width_part = width_part + lax.dot_general(d_up, w_up, minor, preferred_element_type=jnp.float32)
    return (hidden, d_gate, d_up, width_part)


def weight_grads(slot_rows, slot_cot, hidden, d_gate, d_up):
    major = (((0,), (0,)), ((), ()))
    gate_grad = lax.dot_general(
        slot_rows, d_gate, major, preferred_element_type=jnp.float32
    ).astype(jnp.bfloat16)
    up_grad = lax.dot_general(slot_rows, d_up, major, preferred_element_type=jnp.float32).astype(
        jnp.bfloat16
    )
    down_grad = lax.dot_general(hidden, slot_cot, major, preferred_element_type=jnp.float32).astype(
        jnp.bfloat16
    )
    return (gate_grad[None], up_grad[None], down_grad[None])


def local(
    cotangent,
    block_input,
    routes,
    route_weights,
    gate_weight,
    up_weight,
    down_weight,
    out_weight,
    conv_out,
    gate_pre,
    prior_states,
    recur_weight,
    input_gate_matrix,
    decay_param,
    decay_jump,
):
    experts = lax.axis_size("sp")
    tok_rows = cotangent.shape[0]
    capacity = 5 * tok_rows * TOP_K // (4 * experts)
    route_hits = routing_tables(routes, experts, capacity)
    placing = jnp.sum(route_hits.astype(jnp.int32), axis=0).astype(jnp.bfloat16)
    hit_table = route_hits.astype(jnp.bfloat16)
    sent_rows, sent_cot = spread(placing, hit_table, block_input, cotangent, route_weights)
    part_rows, portion_adjoint = (
        lax.all_to_all(
            sent_rows.reshape(experts, capacity, -1), "sp", split_axis=0, concat_axis=0, tiled=True
        ),
        lax.all_to_all(
            sent_cot.reshape(experts, capacity, -1), "sp", split_axis=0, concat_axis=0, tiled=True
        ),
    )
    got_rows, got_cot = (
        lax.all_gather(part_rows, "tp", axis=2, tiled=True),
        lax.all_gather(portion_adjoint, "tp", axis=2, tiled=True),
    )
    full_width = got_rows.shape[2]
    slot_rows = got_rows.reshape(-1, full_width)
    slot_cot = got_cot.reshape(-1, full_width)
    hidden, d_gate, d_up, width_part = expert_work(
        slot_rows, slot_cot, gate_weight[0], up_weight[0], down_weight[0]
    )
    gate_grad, up_grad, down_grad = weight_grads(slot_rows, slot_cot, hidden, d_gate, d_up)
    summed = lax.psum_scatter(
        width_part.reshape(experts, capacity, full_width).astype(jnp.bfloat16),
        "tp",
        scatter_dimension=2,
        tiled=True,
    )
    handed_result = lax.all_to_all(summed, "sp", split_axis=0, concat_axis=0, tiled=True).reshape(
        experts * capacity, -1
    )
    moe_grad = lax.dot_general(
        placing, handed_result, (((0,), (0,)), ((), ())), preferred_element_type=jnp.float32
    )
    block_grad = (cotangent.astype(jnp.float32) + moe_grad).astype(jnp.bfloat16)
    full_grad = lax.all_gather(block_grad, "tp", axis=1, tiled=True)
    channels = conv_out.shape[0]
    length = conv_out.shape[1]
    head_count = channels // HEAD_DIM
    head_start = lax.axis_index("tp") * head_count
    w_recur = lax.dynamic_slice_in_dim(recur_weight, head_start, head_count, 0)
    w_input = lax.dynamic_slice_in_dim(input_gate_matrix, head_start, head_count, 0)
    rate_parameter = lax.dynamic_slice_in_dim(decay_param, head_start * HEAD_DIM, channels, 0)[
        :, None
    ]
    shaped = conv_out.reshape(head_count, HEAD_DIM, length)
    recur_gate = jax.nn.sigmoid(
        jnp.einsum("hij,hit->hjt", w_recur, shaped, preferred_element_type=jnp.float32).reshape(
            channels, length
        )
    )
    input_gate = jax.nn.sigmoid(
        jnp.einsum("hij,hit->hjt", w_input, shaped, preferred_element_type=jnp.float32).reshape(
            channels, length
        )
    )
    softened = jax.nn.softplus(-rate_parameter)
    log_decay = -RATE_SCALE * recur_gate * softened + decay_jump
    decay_val = jnp.exp(log_decay)
    norm_scale = jnp.sqrt(-jnp.expm1(2.0 * log_decay))
    conv_vals = conv_out.astype(jnp.float32)
    prior_vals = prior_states.astype(jnp.float32)
    state = decay_val * prior_vals + norm_scale * input_gate * conv_vals
    gelu_val, gelu_pull = jax.vjp(jax.nn.gelu, gate_pre.astype(jnp.float32))
    mixed = (gelu_val * state).astype(jnp.bfloat16)
    d_mixed = lax.dot_general(
        out_weight, full_grad, (((1,), (1,)), ((), ())), preferred_element_type=jnp.float32
    )
    valve_logit_derivative = gelu_pull(d_mixed * state)[0].astype(jnp.bfloat16)
    d_state = d_mixed * gelu_val
    shifted = jnp.concatenate([decay_val[:, 1:], jnp.ones((channels, 1), jnp.float32)], axis=1)
    flipped = lax.associative_scan(link_pairs, (jnp.flip(shifted, 1), jnp.flip(d_state, 1)), axis=1)
    decay_prod = jnp.flip(flipped[0], 1)
    local_sum = jnp.flip(flipped[1], 1)
    summary = (decay_val[:, 0] * decay_prod[:, 0], decay_val[:, 0] * local_sum[:, 0])
    carried = prefix(
        summary,
        "sp",
        later_first,
        (jnp.ones((channels,), jnp.float32), jnp.zeros((channels,), jnp.float32)),
    )[1]
    state_grad = local_sum + decay_prod * carried[:, None]
    grad_log = (
        state_grad * prior_vals * decay_val
        - state_grad * input_gate * conv_vals * decay_val * decay_val / norm_scale
    )
    grad_recur = (grad_log * -RATE_SCALE * softened * recur_gate * (1.0 - recur_gate)).astype(
        jnp.bfloat16
    )
    grad_input = (state_grad * norm_scale * conv_vals * input_gate * (1.0 - input_gate)).astype(
        jnp.bfloat16
    )
    back_recur = jnp.einsum(
        "hij,hjt->hit",
        w_recur,
        grad_recur.reshape(head_count, HEAD_DIM, length),
        preferred_element_type=jnp.float32,
    ).reshape(channels, length)
    back_input = jnp.einsum(
        "hij,hjt->hit",
        w_input,
        grad_input.reshape(head_count, HEAD_DIM, length),
        preferred_element_type=jnp.float32,
    ).reshape(channels, length)
    conv_grad = (state_grad * norm_scale * input_gate + back_recur + back_input).astype(
        jnp.bfloat16
    )
    projected = lax.psum_scatter(
        lax.dot_general(
            full_grad, mixed, (((0,), (1,)), ((), ())), preferred_element_type=jnp.float32
        ).astype(jnp.bfloat16),
        "sp",
        scatter_dimension=0,
        tiled=True,
    ).astype(jnp.float32)
    out_weight_grad = jnp.transpose(projected)
    return (gate_grad, up_grad, down_grad, out_weight_grad, conv_grad, valve_logit_derivative)


def solution(mesh):
    in_specs = (
        P("sp", "tp"),
        P("sp", "tp"),
        P("sp", None),
        P("sp", None),
        P("sp", None, "tp"),
        P("sp", None, "tp"),
        P("sp", "tp", None),
        P("tp", None),
        P("tp", "sp"),
        P("tp", "sp"),
        P("tp", "sp"),
        P(),
        P(),
        P(),
        P("tp", "sp"),
    )
    out_specs = (
        P("sp", None, "tp"),
        P("sp", None, "tp"),
        P("sp", "tp", None),
        P("tp", "sp"),
        P("tp", "sp"),
        P("tp", "sp"),
    )
    return jax.shard_map(local, mesh=mesh, in_specs=in_specs, out_specs=out_specs, check_vma=False)
```

profile of v0, /device:TPU:0, one launch (start us, length us, event | category | flops | bytes accessed | tf_op | source)
XLA Modules:
  0.0 229.2 jit_solution(16892057116044407689)
XLA Ops:
  7.2 0.0 all-gather.6.cloned.1.call-start
  7.2 0.9 copy.72
  8.1 0.1 eq.42
  8.3 0.1 eq.38
  8.4 1.2 reduce-window.6
  9.7 0.2 slice_reduce_fusion
  9.9 0.2 reduce-window.9
  10.1 0.1 add_bitcast_fusion
  10.2 0.1 reduce_sum.21
  10.3 0.1 copy.74
  10.4 0.7 add_bitcast_fusion.1
  11.1 0.3 convert_reduce_fusion
  11.3 1.1 convolution_convert_fusion.1
  12.5 11.7 %all_to_all.15 = bf16[4,160,256]{2,1,0:T(8,128)(2,1)} all-to-all(bf16[4,160,256]{2,1,0:T(8,128)(2,1)S(1)} %bitcast.101), channel_id=1, replica_groups=mesh['sp'=4,'tp'=8] {'sp'}, dimensions={0} | all-to-all | bytes 655360 | tf_op jit(solution)/shard_map/all_to_all | solution.py:113
  24.2 0.0 all-gather.8.cloned.1.call-start
  24.3 0.5 fusion.16
  24.8 9.3 %all_to_all.16 = bf16[4,160,256]{2,1,0:T(8,128)(2,1)} all-to-all(bf16[4,160,256]{2,1,0:T(8,128)(2,1)S(1)} %bitcast.104), channel_id=1, replica_groups=mesh['sp'=4,'tp'=8] {'sp'}, dimensions={0} | all-to-all | bytes 655360 | tf_op jit(solution)/shard_map/all_to_all | solution.py:116
  34.1 0.0 reduce-scatter.3.cloned.1.call-start
  34.2 24.6 %all-gather.6.cloned.1.call-done = bf16[4,160,2048]{2,1,0:T(8,128)(2,1)} async-done(((bf16[4,160,256]{2,1,0:T(8,128)(2,1)}), bf16[4,160,2048]{2,1,0:T(8,128)(2,1)}) %all-gather.6.cloned.1.call-update) | async-done | bytes 2621456 | tf_op jit(solution)/shard_map/all_gather | solution.py:121
  58.8 7.2 %fusion.3 = f32[640,896]{1,0:T(8,128)} fusion(bf16[640,2048]{1,0:T(8,128)(2,1)} %bitcast.114, bf16[1,2048,896]{2,1,0:T(8,128)(2,1)} %param.21), kind=kOutput, calls=%fused_computation.7 | convolution fusion | flops 2348810240 | bytes 8585216 | tf_op jit(solution)/shard_map/dot_general | solution.py:59
  66.0 4.3 %fusion.7 = f32[640,896]{1,0:T(8,128)} fusion(bf16[640,2048]{1,0:T(8,128)(2,1)S(1)} %bitcast.116, bf16[1,2048,896]{2,1,0:T(8,128)(2,1)S(1)} %copy-done.8), kind=kOutput, calls=%fused_computation.11 | convolution fusion | flops 2348810240 | bytes 8585216 | tf_op jit(solution)/shard_map/dot_general | solution.py:60
  70.4 23.2 %all-gather.8.cloned.1.call-done = bf16[4,160,2048]{2,1,0:T(8,128)(2,1)} async-done(((bf16[4,160,256]{2,1,0:T(8,128)(2,1)}), bf16[4,160,2048]{2,1,0:T(8,128)(2,1)}) %all-gather.8.cloned.1.call-update) | async-done | bytes 2621456 | tf_op jit(solution)/shard_map/all_gather | solution.py:122
  93.6 7.8 %multiply_convert_fusion.1 = (bf16[640,896]{1,0:T(8,128)(2,1)S(1)}, bf16[640,896]{1,0:T(8,128)(2,1)S(1)}) fusion(f32[640,896]{1,0:T(8,128)} %fusion.3, f32[640,896]{1,0:T(8,128)} %fusion.7, bf16[640,2048]{1,0:T(8,128)(2,1)} %bitcast.118, bf16[1,896,2048]{2,1,0:T(8,128)(2,1)} %param.23), kind=kOutput, calls=%fused_computation.20 | convolution fusion | flops 2356264960 | bytes 13172736 | tf_op jit(solution)/shard_map/dot_general | solution.py:64
  101.5 2.9 %fusion.1 = f32[640,2048]{1,0:T(8,128)S(1)} fusion(bf16[640,896]{1,0:T(8,128)(2,1)S(1)} %get-tuple-element.152, bf16[1,2048,896]{2,1,0:T(8,128)(2,1)S(1)} %copy-done.7), kind=kOutput, calls=%fused_computation.5 | convolution fusion | flops 2348810240 | bytes 10059776 | tf_op jit(solution)/shard_map/dot_general | solution.py:69
  104.4 4.2 %add_convert_fusion = bf16[640,2048]{1,0:T(8,128)(2,1)} fusion(f32[640,2048]{1,0:T(8,128)S(1)} %fusion.1, bf16[640,896]{1,0:T(8,128)(2,1)S(1)} %get-tuple-element.151, bf16[1,2048,896]{2,1,0:T(8,128)(2,1)S(1)} %copy-done.9), kind=kOutput, calls=%fused_computation.4 | convolution fusion | flops 2351431680 | bytes 12681216 | tf_op jit(solution)/shard_map/dot_general | solution.py:70
  108.6 0.8 copy-done.4
  109.4 0.1 copy.82
  109.5 1.0 fusion.23
  110.6 0.1 copy.81
  110.7 34.2 %reduce-scatter.3.cloned.1.call-done = bf16[4,160,256]{2,1,0:T(8,128)(2,1)} async-done(((bf16[4,160,2048]{2,1,0:T(8,128)(2,1)}), bf16[4,160,256]{2,1,0:T(8,128)(2,1)}) %reduce-scatter.3.cloned.1.call-update) | async-done | bytes 327696 | tf_op jit(solution)/shard_map/reduce_scatter | solution.py:131
  144.9 3.7 %all-to-all-start.2 = ((bf16[4,160,256]{2,1,0:T(8,128)(2,1)}), bf16[4,160,256]{2,1,0:T(8,128)(2,1)S(1)}, u32[]{:S(2)}, u32[]{:S(2)}) async-start(bf16[4,160,256]{2,1,0:T(8,128)(2,1)} %reduce-scatter.3.cloned.1.call-done), calls=%async_computation.3 | async-start | bytes 655360 | tf_op jit(solution)/shard_map/all_to_all | solution.py:137
  148.5 0.0 all-gather.10.cloned.1.call-start
  148.6 1.0 fusion.21
  149.6 0.1 copy.77
  149.7 0.1 copy.79
  149.8 0.1 copy.75
  149.9 0.1 copy.78
  150.0 0.8 fusion.70
  150.8 3.3 %all-to-all-done.2 = bf16[4,160,256]{2,1,0:T(8,128)(2,1)S(1)} async-done(((bf16[4,160,256]{2,1,0:T(8,128)(2,1)}), bf16[4,160,256]{2,1,0:T(8,128)(2,1)S(1)}, u32[]{:S(2)}, u32[]{:S(2)}) %all-to-all-start.2) | async-done | bytes 327712 | tf_op jit(solution)/shard_map/all_to_all | solution.py:137
  154.1 1.0 fusion.17
  155.1 0.0 reduce-scatter.5.cloned.1.call-start
  155.1 7.4 %convert_bitcast_fusion.1 = bf16[1,2048,896]{2,1,0:T(8,128)(2,1)} fusion(bf16[640,2048]{1,0:T(8,128)(2,1)} %bitcast.115, bf16[640,896]{1,0:T(8,128)(2,1)} %copy-done.18), kind=kOutput, calls=%fused_computation.16 | convolution fusion | flops 2350645248 | bytes 7438336 | tf_op jit(solution)/shard_map/dot_general | solution.py:79
  162.6 4.9 %convert_bitcast_fusion.2 = bf16[1,2048,896]{2,1,0:T(8,128)(2,1)} fusion(bf16[640,2048]{1,0:T(8,128)(2,1)S(1)} %bitcast.117, bf16[640,896]{1,0:T(8,128)(2,1)S(1)} %copy-done.15), kind=kOutput, calls=%fused_computation.17 | convolution fusion | flops 2350645248 | bytes 7438336 | tf_op jit(solution)/shard_map/dot_general | solution.py:76
  167.5 4.6 %convert_bitcast_fusion = bf16[1,896,2048]{2,1,0:T(8,128)(2,1)} fusion(bf16[640,2048]{1,0:T(8,128)(2,1)S(1)} %bitcast.119, f32[640,896]{1,0:T(8,128)S(1)} %copy-done.17, f32[640,896]{1,0:T(8,128)S(1)} %copy-done.16), kind=kOutput, calls=%fused_computation.15 | convolution fusion | flops 2354085888 | bytes 10878976 | tf_op jit(solution)/shard_map/dot_general | solution.py:82
  172.1 4.3 %all-gather.10.cloned.1.call-done = bf16[256,2048]{1,0:T(8,128)(2,1)} async-done(((bf16[256,256]{1,0:T(8,128)(2,1)}), bf16[256,2048]{1,0:T(8,128)(2,1)}) %all-gather.10.cloned.1.call-update) | async-done | bytes 1048592 | tf_op jit(solution)/shard_map/all_gather | solution.py:144
  176.4 1.7 fusion.40
  180.3 7.2 %all-gather = f32[512,1]{0,1:T(1,128)S(1)} all-gather(f32[128,1]{0,1:T(1,128)S(1)} %get-tuple-element.156), channel_id=2, replica_groups=mesh['sp'=4,'tp'=8] {'sp'}, dimensions={0}, use_global_device_ids=true | all-gather | bytes 2560 | tf_op jit(solution)/shard_map/all_gather | solution.py:13
  187.5 7.9 %all-gather.1 = f32[512,1]{0,1:T(1,128)S(1)} all-gather(f32[128,1]{0,1:T(1,128)S(1)} %get-tuple-element.155), channel_id=3, replica_groups=mesh['sp'=4,'tp'=8] {'sp'}, dimensions={0}, use_global_device_ids=true | all-gather | bytes 2560 | tf_op jit(solution)/shard_map/all_gather | solution.py:13
  195.4 1.4 convolution_convert_fusion
  196.8 0.1 while.14
  197.0 0.1 rev.16
  197.1 0.1 rev.15
  197.2 0.2 fusion.43
  197.4 0.1 copy.87
  197.5 0.9 fusion.62
  198.4 0.1 copy.89
  198.5 0.1 copy.92
  198.6 0.9 fusion.59
  199.5 0.1 copy.94
  199.7 0.7 copy.96
  200.4 0.7 copy.97
  201.1 19.8 %reduce-scatter.5.cloned.1.call-done = bf16[512,128]{1,0:T(8,128)(2,1)} async-done(((bf16[2048,128]{1,0:T(8,128)(2,1)}), bf16[512,128]{1,0:T(8,128)(2,1)}) %reduce-scatter.5.cloned.1.call-update) | async-done | bytes 131088 | tf_op jit(solution)/shard_map/reduce_scatter | solution.py:216
  220.9 0.9 convert_bitcast_fusion.3
  221.8 0.8 copy.95
  (185 shorter events, 1.8 us)
Async XLA Ops:
  7.2 169.2 %copy-start = (bf16[128,2048]{1,0:T(8,128)(2,1)S(1)}, bf16[128,2048]{1,0:T(8,128)(2,1)}, u32[]{:S(2)}) copy-start(bf16[128,2048]{1,0:T(8,128)(2,1)} %param.24) | copy-start | bytes 1572868
  7.2 17.1 %copy-start.2 = (bf16[256,256]{1,0:T(8,128)(2,1)S(1)}, bf16[256,256]{1,0:T(8,128)(2,1)}, u32[]{:S(2)}) copy-start(bf16[256,256]{1,0:T(8,128)(2,1)} %param.17) | copy-start | bytes 393220
  7.2 17.1 %copy-start.13 = (f32[256,2]{0,1:T(2,128)S(1)}, f32[256,2]{0,1:T(2,128)}, u32[]{:S(2)}) copy-start(f32[256,2]{0,1:T(2,128)} %param.20) | copy-start | bytes 6148
  7.2 51.6 %all-gather.6.cloned.1.call-start = ((), (), s32[]{:S(2)}) async-start(), calls=%async_computation.5 | async-start | bytes 2949120 | tf_op jit(solution)/shard_map/all_gather | solution.py:121
  24.2 69.4 %all-gather.8.cloned.1.call-start = ((), (), s32[]{:S(2)}) async-start(), calls=%async_computation.6 | async-start | bytes 2949120 | tf_op jit(solution)/shard_map/all_gather | solution.py:122
  34.1 110.8 %reduce-scatter.3.cloned.1.call-start = ((), (), s32[]{:S(2)}) async-start(), calls=%async_computation.7 | async-start | bytes 2949120 | tf_op jit(solution)/shard_map/reduce_scatter | solution.py:131
  58.8 7.2 %copy-start.8 = (bf16[1,2048,896]{2,1,0:T(8,128)(2,1)S(1)}, bf16[1,2048,896]{2,1,0:T(8,128)(2,1)}, u32[]{:S(2)}) copy-start(bf16[1,2048,896]{2,1,0:T(8,128)(2,1)} %param.22) | copy-start | bytes 11010052
  58.8 7.2 %copy-start.10 = (bf16[4,160,2048]{2,1,0:T(8,128)(2,1)S(1)}, bf16[4,160,2048]{2,1,0:T(8,128)(2,1)}, u32[]{:S(2)}) copy-start(bf16[4,160,2048]{2,1,0:T(8,128)(2,1)} %all-gather.6.cloned.1.call-done) | copy-start | bytes 7864324
  93.6 7.8 %copy-start.7 = (bf16[1,2048,896]{2,1,0:T(8,128)(2,1)S(1)}, bf16[1,2048,896]{2,1,0:T(8,128)(2,1)}, u32[]{:S(2)}) copy-start(bf16[1,2048,896]{2,1,0:T(8,128)(2,1)} %param.21) | copy-start | bytes 11010052
  101.4 3.0 %copy-start.14 = (bf16[640,896]{1,0:T(8,128)(2,1)}, bf16[640,896]{1,0:T(8,128)(2,1)S(1)}, u32[]{:S(2)}) copy-start(bf16[640,896]{1,0:T(8,128)(2,1)S(1)} %get-tuple-element.152) | copy-start | bytes 3440644
  101.4 3.0 %copy-start.18 = (bf16[640,896]{1,0:T(8,128)(2,1)}, bf16[640,896]{1,0:T(8,128)(2,1)S(1)}, u32[]{:S(2)}) copy-start(bf16[640,896]{1,0:T(8,128)(2,1)S(1)} %get-tuple-element.151) | copy-start | bytes 3440644
  101.4 2.9 %copy-start.9 = (bf16[1,2048,896]{2,1,0:T(8,128)(2,1)S(1)}, bf16[1,2048,896]{2,1,0:T(8,128)(2,1)}, u32[]{:S(2)}) copy-start(bf16[1,2048,896]{2,1,0:T(8,128)(2,1)} %param.22) | copy-start | bytes 11010052
  108.6 0.8 copy-start.4
  108.6 41.1 %copy-start.5 = (bf16[128,256]{1,0:T(8,128)(2,1)S(1)}, bf16[128,256]{1,0:T(8,128)(2,1)}, u32[]{:S(2)}) copy-start(bf16[128,256]{1,0:T(8,128)(2,1)} %param.27) | copy-start | bytes 196612
  108.6 41.2 %copy-start.6 = (bf16[128,256]{1,0:T(8,128)(2,1)S(1)}, bf16[128,256]{1,0:T(8,128)(2,1)}, u32[]{:S(2)}) copy-start(bf16[128,256]{1,0:T(8,128)(2,1)} %param.26) | copy-start | bytes 196612
  108.6 41.3 %copy-start.3 = (f32[128,256]{1,0:T(8,128)S(1)}, f32[128,256]{1,0:T(8,128)}, u32[]{:S(2)}) copy-start(f32[128,256]{1,0:T(8,128)} %param.31) | copy-start | bytes 393220
  144.9 9.2 %all-to-all-start.2 = ((bf16[4,160,256]{2,1,0:T(8,128)(2,1)}), bf16[4,160,256]{2,1,0:T(8,128)(2,1)S(1)}, u32[]{:S(2)}, u32[]{:S(2)}) async-start(bf16[4,160,256]{2,1,0:T(8,128)(2,1)} %reduce-scatter.3.cloned.1.call-done), calls=%async_computation.3 | async-start | bytes 655360 | tf_op jit(solution)/shard_map/all_to_all | solution.py:137
  148.5 27.9 %all-gather.10.cloned.1.call-start = ((), (), s32[]{:S(2)}) async-start(), calls=%async_computation.8 | async-start | bytes 1179648 | tf_op jit(solution)/shard_map/all_gather | solution.py:144
  155.1 7.5 %copy-start.15 = (bf16[640,896]{1,0:T(8,128)(2,1)S(1)}, bf16[640,896]{1,0:T(8,128)(2,1)}, u32[]{:S(2)}) copy-start(bf16[640,896]{1,0:T(8,128)(2,1)} %copy-done.14) | copy-start | bytes 3440644
  155.1 65.8 %reduce-scatter.5.cloned.1.call-start = ((), (), s32[]{:S(2)}) async-start(), calls=%async_computation.9 | async-start | bytes 655360 | tf_op jit(solution)/shard_map/reduce_scatter | solution.py:216
  155.1 7.4 %copy-start.11 = (bf16[4,160,2048]{2,1,0:T(8,128)(2,1)S(1)}, bf16[4,160,2048]{2,1,0:T(8,128)(2,1)}, u32[]{:S(2)}) copy-start(bf16[4,160,2048]{2,1,0:T(8,128)(2,1)} %all-gather.6.cloned.1.call-done) | copy-start | bytes 7864324
  162.5 4.9 %copy-start.12 = (bf16[4,160,2048]{2,1,0:T(8,128)(2,1)S(1)}, bf16[4,160,2048]{2,1,0:T(8,128)(2,1)}, u32[]{:S(2)}) copy-start(bf16[4,160,2048]{2,1,0:T(8,128)(2,1)} %all-gather.8.cloned.1.call-done) | copy-start | bytes 7864324
  162.5 4.9 %copy-start.16 = (f32[640,896]{1,0:T(8,128)S(1)}, f32[640,896]{1,0:T(8,128)}, u32[]{:S(2)}) copy-start(f32[640,896]{1,0:T(8,128)} %fusion.3) | copy-start | bytes 6881284
  162.6 4.9 %copy-start.17 = (f32[640,896]{1,0:T(8,128)S(1)}, f32[640,896]{1,0:T(8,128)}, u32[]{:S(2)}) copy-start(f32[640,896]{1,0:T(8,128)} %fusion.7) | copy-start | bytes 6881284
  178.5 16.9 %copy-start.1 = (bf16[256,2048]{1,0:T(8,128)(2,1)S(1)}, bf16[256,2048]{1,0:T(8,128)(2,1)}, u32[]{:S(2)}) copy-start(bf16[256,2048]{1,0:T(8,128)(2,1)} %all-gather.10.cloned.1.call-done) | copy-start | bytes 3145732
Sparse Core Ops, SparseCore 0:
  24.3 34.4 all-gather.5
  60.4 33.1 all-gather.7
  108.7 36.0 reduce-scatter.2
  155.2 21.1 all-gather.9
  196.9 23.9 reduce-scatter.4
where the time goes:
time: 230 us; the launch traced here: 229 us
  waiting for transfers between devices  110 us (48%)
  matrix products  52.8 us (23%)
  blocking collectives  36 us (16%)
  between operations  14.9 us (6%)
  local copies, waits for them, and re-layouts  7.07 us (3%)
  other arithmetic  4.91 us (2%)
  starting transfers between devices  3.85 us (2%)
    reduce_scatter x1, waiting for transfers between devices, local(): lax.psum_scatter(width_part.reshape(experts, capacity, full_width).astype...  34.2 us
    all_gather x1, waiting for transfers between devices, local(): lax.all_gather(part_rows, 'tp', axis=2, tiled=True)  24.6 us
    all_gather x1, waiting for transfers between devices, local(): lax.all_gather(portion_adjoint, 'tp', axis=2, tiled=True)  23.2 us
    reduce_scatter x1, waiting for transfers between devices, local(): lax.psum_scatter(lax.dot_general(full_grad, mixed, (((0,), (1,)), ((), ()...  19.8 us
    all_gather x2, blocking collectives, prefix(): pieces = jax.tree.map(lambda part: lax.all_gather(part, axis), value)  15 us
    all_to_all x1, blocking collectives, local(): lax.all_to_all(sent_rows.reshape(experts, capacity, -1), 'sp', split_axis...  11.7 us
    all_to_all x1, blocking collectives, local(): lax.all_to_all(sent_cot.reshape(experts, capacity, -1), 'sp', split_axis=...  9.32 us
    dot_general x1, matrix products, expert_work(): lax.dot_general(slot_cot, w_down, minor, preferred_element_type=jnp.float32)  7.79 us
  transfers between devices with their start and end apart: 6, of which 6 were waited for; matrix products, arithmetic and copies ran while one was open for 16% of the time, Pallas kernels for 0%

commit v1 on v0

--- a/solution.py
+++ b/solution.py
@@ -119,7 +119,9 @@
     )
     got_rows, got_cot = (
         lax.all_gather(part_rows, "tp", axis=2, tiled=True),
-        lax.all_gather(portion_adjoint, "tp", axis=2, tiled=True),
+        jnp.concatenate(
+            lax.all_to_all(jnp.stack([portion_adjoint] * lax.axis_size("tp")), "tp", 0, 0), axis=2
+        ),
     )
     full_width = got_rows.shape[2]
     slot_rows = got_rows.reshape(-1, full_width)

time: 230 us -> 250 us (1.087)
  waiting for transfers between devices: 110 us -> 123 us
  local copies, waits for them, and re-layouts: 7.07 us -> 13.8 us
  starting transfers between devices: 3.85 us -> 8.63 us
  matrix products: 52.8 us -> 48.7 us
    all_to_all x0 -> x1, waiting for transfers between devices: none -> 26.6 us  [local(): lax.all_to_all(jnp.stack([portion_adjoint] * lax.axis_size('tp')), 'tp',...]
    all_gather x1 -> x0, waiting for transfers between devices: 23.2 us -> none  [local(): lax.all_gather(portion_adjoint, 'tp', axis=2, tiled=True)]
    all_gather x1, waiting for transfers between devices: 24.6 us -> 35.1 us  [local(): lax.all_gather(part_rows, 'tp', axis=2, tiled=True)]
    all_to_all x0 -> x1, starting transfers between devices: none -> 4.87 us  [local(): lax.all_to_all(jnp.stack([portion_adjoint] * lax.axis_size('tp')), 'tp',...]
    dot_general x1, matrix products: 7.79 us -> 3.54 us  [expert_work(): lax.dot_general(slot_cot, w_down, minor, preferred_element_type=jnp.float32)]
    unnamed x46 -> x59, local copies, waits for them, and re-layouts: 4.49 us -> 7.89 us
  transfers between devices with their start and end apart: 6 -> 6, of which waited for: 6 -> 6; matrix products, arithmetic and copies ran while one was open for 16% -> 15% of each run, Pallas kernels for 0% -> 0%
where the time goes in v1:
time: 250 us; the launch traced here: 249 us
  waiting for transfers between devices  123 us (49%)
  matrix products  48.7 us (19%)
  blocking collectives  35.4 us (14%)
  between operations  14.9 us (6%)
  local copies, waits for them, and re-layouts  13.8 us (6%)
  starting transfers between devices  8.63 us (3%)
  other arithmetic  4.89 us (2%)
    all_gather x1, waiting for transfers between devices, local(): lax.all_gather(part_rows, 'tp', axis=2, tiled=True)  35.1 us
    reduce_scatter x1, waiting for transfers between devices, local(): lax.psum_scatter(width_part.reshape(experts, capacity, full_width).astype...  34 us
    all_to_all x1, waiting for transfers between devices, local(): lax.all_to_all(jnp.stack([portion_adjoint] * lax.axis_size('tp')), 'tp',...  26.6 us
    reduce_scatter x1, waiting for transfers between devices, local(): lax.psum_scatter(lax.dot_general(full_grad, mixed, (((0,), (1,)), ((), ()...  19.8 us
    all_gather x2, blocking collectives, prefix(): pieces = jax.tree.map(lambda part: lax.all_gather(part, axis), value)  15 us
    all_to_all x1, blocking collectives, local(): lax.all_to_all(sent_rows.reshape(experts, capacity, -1), 'sp', split_axis...  11.7 us
    all_to_all x1, blocking collectives, local(): lax.all_to_all(sent_cot.reshape(experts, capacity, -1), 'sp', split_axis=...  8.62 us
    unnamed x59, local copies, waits for them, and re-layouts  7.89 us
  transfers between devices with their start and end apart: 6, of which 6 were waited for; matrix products, arithmetic and copies ran while one was open for 15% of the time, Pallas kernels for 0%

profile of v1, /device:TPU:0, one launch (start us, length us, event | category | flops | bytes accessed | tf_op | source)
XLA Modules:
  0.0 249.5 jit_solution(7711154814992926171)
XLA Ops:
  7.2 0.9 copy.101
  8.1 0.1 eq.42
  8.3 0.1 eq.38
  8.4 1.2 reduce-window.6
  9.7 0.2 slice_reduce_fusion
  9.9 0.2 reduce-window.9
  10.1 0.1 add_bitcast_fusion
  10.2 0.1 reduce_sum.21
  10.4 0.7 add_bitcast_fusion.1
  11.1 0.3 convert_reduce_fusion
  11.4 0.9 copy-done.1
  12.2 1.1 convolution_convert_fusion.1
  13.4 11.7 %all_to_all.20 = bf16[4,160,256]{2,1,0:T(8,128)(2,1)} all-to-all(bf16[4,160,256]{2,1,0:T(8,128)(2,1)S(1)} %bitcast.108), channel_id=1, replica_groups=mesh['sp'=4,'tp'=8] {'sp'}, dimensions={0} | all-to-all | bytes 655360 | tf_op jit(solution)/shard_map/all_to_all | solution.py:113
  25.2 0.5 fusion.16
  25.6 8.6 %all_to_all.21 = bf16[4,160,256]{2,1,0:T(8,128)(2,1)S(1)} all-to-all(bf16[4,160,256]{2,1,0:T(8,128)(2,1)S(1)} %bitcast.111), channel_id=1, replica_groups=mesh['sp'=4,'tp'=8] {'sp'}, dimensions={0} | all-to-all | bytes 655360 | tf_op jit(solution)/shard_map/all_to_all | solution.py:116
  34.2 1.8 stack.2
  36.0 4.9 %all-to-all-start.2 = ((bf16[8,4,160,256]{3,2,1,0:T(8,128)(2,1)}), bf16[8,4,160,256]{3,2,1,0:T(8,128)(2,1)S(1)}, u32[]{:S(2)}, u32[]{:S(2)}) async-start(bf16[8,4,160,256]{3,2,1,0:T(8,128)(2,1)} %stack.2), calls=%async_computation.2 | async-start | bytes 5242880 | tf_op jit(solution)/shard_map/all_to_all | solution.py:123
  40.9 35.1 %all-gather.5.cloned.1.call-done = bf16[4,160,2048]{2,1,0:T(8,128)(2,1)} async-done(((bf16[4,160,256]{2,1,0:T(8,128)(2,1)}), bf16[4,160,2048]{2,1,0:T(8,128)(2,1)}) %all-gather.5.cloned.1.call-update) | async-done | bytes 2621456 | tf_op jit(solution)/shard_map/all_gather | solution.py:121
  76.0 7.3 %fusion.3 = f32[640,896]{1,0:T(8,128)} fusion(bf16[640,2048]{1,0:T(8,128)(2,1)} %bitcast.121, bf16[1,2048,896]{2,1,0:T(8,128)(2,1)} %param.21), kind=kOutput, calls=%fused_computation.7 | convolution fusion | flops 2348810240 | bytes 8585216 | tf_op jit(solution)/shard_map/dot_general | solution.py:59
  83.3 4.3 %fusion.7 = f32[640,896]{1,0:T(8,128)} fusion(bf16[640,2048]{1,0:T(8,128)(2,1)S(1)} %bitcast.123, bf16[1,2048,896]{2,1,0:T(8,128)(2,1)S(1)} %copy-done.13), kind=kOutput, calls=%fused_computation.11 | convolution fusion | flops 2348810240 | bytes 8585216 | tf_op jit(solution)/shard_map/dot_general | solution.py:60
  87.6 26.6 %all-to-all-done.2 = bf16[8,4,160,256]{3,2,1,0:T(8,128)(2,1)S(1)} async-done(((bf16[8,4,160,256]{3,2,1,0:T(8,128)(2,1)}), bf16[8,4,160,256]{3,2,1,0:T(8,128)(2,1)S(1)}, u32[]{:S(2)}, u32[]{:S(2)}) %all-to-all-start.2) | async-done | bytes 2621472 | tf_op jit(solution)/shard_map/all_to_all | solution.py:123
  114.2 1.5 copy.104
  115.7 0.9 copy.133
  116.6 1.6 copy-done.11
  118.2 3.5 %multiply_convert_fusion.1 = (bf16[640,896]{1,0:T(8,128)(2,1)S(1)}, bf16[640,896]{1,0:T(8,128)(2,1)S(1)}) fusion(f32[640,896]{1,0:T(8,128)S(1)} %copy-done.20, f32[640,896]{1,0:T(8,128)S(1)} %copy-done.22, bf16[640,2048]{1,0:T(8,128)(2,1)S(1)} %bitcast.104, bf16[1,896,2048]{2,1,0:T(8,128)(2,1)S(1)} %copy-done.11), kind=kOutput, calls=%fused_computation.20 | convolution fusion | flops 2356264960 | bytes 13172736 | tf_op jit(solution)/shard_map/dot_general | solution.py:64
  121.8 2.9 %fusion.1 = f32[640,2048]{1,0:T(8,128)S(1)} fusion(bf16[640,896]{1,0:T(8,128)(2,1)S(1)} %get-tuple-element.158, bf16[1,2048,896]{2,1,0:T(8,128)(2,1)S(1)} %copy-done.12), kind=kOutput, calls=%fused_computation.5 | convolution fusion | flops 2348810240 | bytes 10059776 | tf_op jit(solution)/shard_map/dot_general | solution.py:69
  124.8 4.4 %add_convert_fusion = bf16[640,2048]{1,0:T(8,128)(2,1)} fusion(f32[640,2048]{1,0:T(8,128)S(1)} %fusion.1, bf16[640,896]{1,0:T(8,128)(2,1)S(1)} %get-tuple-element.157, bf16[1,2048,896]{2,1,0:T(8,128)(2,1)S(1)} %copy-done.14), kind=kOutput, calls=%fused_computation.4 | convolution fusion | flops 2351431680 | bytes 12681216 | tf_op jit(solution)/shard_map/dot_general | solution.py:70
  129.2 0.8 copy-done.8
  130.0 0.1 copy.112
  130.1 1.0 fusion.23
  131.1 0.1 copy.111
  131.2 34.0 %reduce-scatter.3.cloned.1.call-done = bf16[4,160,256]{2,1,0:T(8,128)(2,1)} async-done(((bf16[4,160,2048]{2,1,0:T(8,128)(2,1)}), bf16[4,160,256]{2,1,0:T(8,128)(2,1)}) %reduce-scatter.3.cloned.1.call-update) | async-done | bytes 327696 | tf_op jit(solution)/shard_map/reduce_scatter | solution.py:133
  165.2 3.6 %all-to-all-start.3 = ((bf16[4,160,256]{2,1,0:T(8,128)(2,1)}), bf16[4,160,256]{2,1,0:T(8,128)(2,1)S(1)}, u32[]{:S(2)}, u32[]{:S(2)}) async-start(bf16[4,160,256]{2,1,0:T(8,128)(2,1)} %reduce-scatter.3.cloned.1.call-done), calls=%async_computation.4 | async-start | bytes 655360 | tf_op jit(solution)/shard_map/all_to_all | solution.py:139
  168.8 1.0 fusion.21
  169.8 0.1 copy.107
  170.0 0.1 copy.109
  170.1 0.1 copy.105
  170.2 0.1 copy.108
  170.3 0.8 fusion.70
  171.1 3.3 %all-to-all-done.3 = bf16[4,160,256]{2,1,0:T(8,128)(2,1)S(1)} async-done(((bf16[4,160,256]{2,1,0:T(8,128)(2,1)}), bf16[4,160,256]{2,1,0:T(8,128)(2,1)S(1)}, u32[]{:S(2)}, u32[]{:S(2)}) %all-to-all-start.3) | async-done | bytes 327712 | tf_op jit(solution)/shard_map/all_to_all | solution.py:139
  174.4 1.0 fusion.17
  175.5 7.4 %convert_bitcast_fusion.1 = bf16[1,2048,896]{2,1,0:T(8,128)(2,1)} fusion(bf16[640,2048]{1,0:T(8,128)(2,1)} %bitcast.122, bf16[640,896]{1,0:T(8,128)(2,1)} %copy-done.24), kind=kOutput, calls=%fused_computation.16 | convolution fusion | flops 2350645248 | bytes 7438336 | tf_op jit(solution)/shard_map/dot_general | solution.py:79
  182.9 4.9 %convert_bitcast_fusion.2 = bf16[1,2048,896]{2,1,0:T(8,128)(2,1)} fusion(bf16[640,2048]{1,0:T(8,128)(2,1)S(1)} %bitcast.124, bf16[640,896]{1,0:T(8,128)(2,1)S(1)} %copy-done.19), kind=kOutput, calls=%fused_computation.17 | convolution fusion | flops 2350645248 | bytes 7438336 | tf_op jit(solution)/shard_map/dot_general | solution.py:76
  187.8 4.6 %convert_bitcast_fusion = bf16[1,896,2048]{2,1,0:T(8,128)(2,1)} fusion(bf16[640,2048]{1,0:T(8,128)(2,1)S(1)} %bitcast.105, f32[640,896]{1,0:T(8,128)S(1)} %copy-done.23, f32[640,896]{1,0:T(8,128)S(1)} %copy-done.21), kind=kOutput, calls=%fused_computation.15 | convolution fusion | flops 2354085888 | bytes 10878976 | tf_op jit(solution)/shard_map/dot_general | solution.py:82
  192.4 4.3 %all-gather.7.cloned.1.call-done = bf16[256,2048]{1,0:T(8,128)(2,1)} async-done(((bf16[256,256]{1,0:T(8,128)(2,1)}), bf16[256,2048]{1,0:T(8,128)(2,1)}) %all-gather.7.cloned.1.call-update) | async-done | bytes 1048592 | tf_op jit(solution)/shard_map/all_gather | solution.py:146
  196.7 1.8 fusion.40
  200.6 7.2 %all-gather = f32[512,1]{0,1:T(1,128)S(1)} all-gather(f32[128,1]{0,1:T(1,128)S(1)} %get-tuple-element.162), channel_id=2, replica_groups=mesh['sp'=4,'tp'=8] {'sp'}, dimensions={0}, use_global_device_ids=true | all-gather | bytes 2560 | tf_op jit(solution)/shard_map/all_gather | solution.py:13
  207.7 7.9 %all-gather.1 = f32[512,1]{0,1:T(1,128)S(1)} all-gather(f32[128,1]{0,1:T(1,128)S(1)} %get-tuple-element.161), channel_id=3, replica_groups=mesh['sp'=4,'tp'=8] {'sp'}, dimensions={0}, use_global_device_ids=true | all-gather | bytes 2560 | tf_op jit(solution)/shard_map/all_gather | solution.py:13
  215.7 1.4 convolution_convert_fusion
  217.1 0.1 while.14
  217.3 0.1 rev.16
  217.3 0.1 rev.15
  217.4 0.2 fusion.43
  217.6 0.1 copy.117
  217.8 0.9 fusion.62
  218.7 0.1 copy.119
  218.8 0.1 copy.122
  218.9 0.9 fusion.59
  219.8 0.1 copy.124
  219.9 0.7 copy.126
  220.7 0.7 copy.127
  221.4 19.8 %reduce-scatter.5.cloned.1.call-done = bf16[512,128]{1,0:T(8,128)(2,1)} async-done(((bf16[2048,128]{1,0:T(8,128)(2,1)}), bf16[512,128]{1,0:T(8,128)(2,1)}) %reduce-scatter.5.cloned.1.call-update) | async-done | bytes 131088 | tf_op jit(solution)/shard_map/reduce_scatter | solution.py:218
  241.2 0.9 convert_bitcast_fusion.3
  242.1 0.8 copy.125
  (199 shorter events, 2.0 us)
Async XLA Ops:
  7.2 189.5 %copy-start = (bf16[128,2048]{1,0:T(8,128)(2,1)S(1)}, bf16[128,2048]{1,0:T(8,128)(2,1)}, u32[]{:S(2)}) copy-start(bf16[128,2048]{1,0:T(8,128)(2,1)} %param.24) | copy-start | bytes 1572868
  7.2 17.9 %copy-start.6 = (bf16[256,256]{1,0:T(8,128)(2,1)S(1)}, bf16[256,256]{1,0:T(8,128)(2,1)}, u32[]{:S(2)}) copy-start(bf16[256,256]{1,0:T(8,128)(2,1)} %param.17) | copy-start | bytes 393220
  7.2 18.0 %copy-start.17 = (f32[256,2]{0,1:T(2,128)S(1)}, f32[256,2]{0,1:T(2,128)}, u32[]{:S(2)}) copy-start(f32[256,2]{0,1:T(2,128)} %param.20) | copy-start | bytes 6148
  7.2 68.8 %all-gather.5.cloned.1.call-start = ((), (), s32[]{:S(2)}) async-start(), calls=%async_computation.6 | async-start | bytes 2949120 | tf_op jit(solution)/shard_map/all_gather | solution.py:121
  11.3 0.9 copy-start.1
  36.0 78.1 %all-to-all-start.2 = ((bf16[8,4,160,256]{3,2,1,0:T(8,128)(2,1)}), bf16[8,4,160,256]{3,2,1,0:T(8,128)(2,1)S(1)}, u32[]{:S(2)}, u32[]{:S(2)}) async-start(bf16[8,4,160,256]{3,2,1,0:T(8,128)(2,1)} %stack.2), calls=%async_computation.2 | async-start | bytes 5242880 | tf_op jit(solution)/shard_map/all_to_all | solution.py:123
  40.9 124.3 %reduce-scatter.3.cloned.1.call-start = ((), (), s32[]{:S(2)}) async-start(), calls=%async_computation.7 | async-start | bytes 2949120 | tf_op jit(solution)/shard_map/reduce_scatter | solution.py:133
  76.0 7.3 %copy-start.13 = (bf16[1,2048,896]{2,1,0:T(8,128)(2,1)S(1)}, bf16[1,2048,896]{2,1,0:T(8,128)(2,1)}, u32[]{:S(2)}) copy-start(bf16[1,2048,896]{2,1,0:T(8,128)(2,1)} %param.22) | copy-start | bytes 11010052
  76.0 7.3 %copy-start.15 = (bf16[4,160,2048]{2,1,0:T(8,128)(2,1)S(1)}, bf16[4,160,2048]{2,1,0:T(8,128)(2,1)}, u32[]{:S(2)}) copy-start(bf16[4,160,2048]{2,1,0:T(8,128)(2,1)} %all-gather.5.cloned.1.call-done) | copy-start | bytes 7864324
  114.1 2.4 copy-start.20
  114.2 2.4 copy-start.22
  115.7 2.6 %copy-start.11 = (bf16[1,896,2048]{2,1,0:T(8,128)(2,1)S(1)}, bf16[1,896,2048]{2,1,0:T(8,128)(2,1)}, u32[]{:S(2)}) copy-start(bf16[1,896,2048]{2,1,0:T(8,128)(2,1)} %param.23) | copy-start | bytes 11010052
  116.6 5.2 %copy-start.3 = (bf16[80,8,8,256]{3,1,2,0:T(8,128)(2,1)}, bf16[80,8,8,256]{3,1,2,0:T(8,128)(2,1)S(1)}, u32[]{:S(2)}) copy-start(bf16[80,8,8,256]{3,1,2,0:T(8,128)(2,1)S(1)} %copy.133) | copy-start | bytes 7864324
  118.2 3.6 %copy-start.12 = (bf16[1,2048,896]{2,1,0:T(8,128)(2,1)S(1)}, bf16[1,2048,896]{2,1,0:T(8,128)(2,1)}, u32[]{:S(2)}) copy-start(bf16[1,2048,896]{2,1,0:T(8,128)(2,1)} %param.21) | copy-start | bytes 11010052
  121.8 3.0 %copy-start.18 = (bf16[640,896]{1,0:T(8,128)(2,1)}, bf16[640,896]{1,0:T(8,128)(2,1)S(1)}, u32[]{:S(2)}) copy-start(bf16[640,896]{1,0:T(8,128)(2,1)S(1)} %get-tuple-element.158) | copy-start | bytes 3440644
  121.8 3.0 %copy-start.24 = (bf16[640,896]{1,0:T(8,128)(2,1)}, bf16[640,896]{1,0:T(8,128)(2,1)S(1)}, u32[]{:S(2)}) copy-start(bf16[640,896]{1,0:T(8,128)(2,1)S(1)} %get-tuple-element.157) | copy-start | bytes 3440644
  121.8 2.9 %copy-start.14 = (bf16[1,2048,896]{2,1,0:T(8,128)(2,1)S(1)}, bf16[1,2048,896]{2,1,0:T(8,128)(2,1)}, u32[]{:S(2)}) copy-start(bf16[1,2048,896]{2,1,0:T(8,128)(2,1)} %param.22) | copy-start | bytes 11010052
  129.1 0.8 copy-start.8
  129.1 40.8 %copy-start.9 = (bf16[128,256]{1,0:T(8,128)(2,1)S(1)}, bf16[128,256]{1,0:T(8,128)(2,1)}, u32[]{:S(2)}) copy-start(bf16[128,256]{1,0:T(8,128)(2,1)} %param.27) | copy-start | bytes 196612
  129.1 40.9 %copy-start.10 = (bf16[128,256]{1,0:T(8,128)(2,1)S(1)}, bf16[128,256]{1,0:T(8,128)(2,1)}, u32[]{:S(2)}) copy-start(bf16[128,256]{1,0:T(8,128)(2,1)} %param.26) | copy-start | bytes 196612
  129.1 41.1 %copy-start.7 = (f32[128,256]{1,0:T(8,128)S(1)}, f32[128,256]{1,0:T(8,128)}, u32[]{:S(2)}) copy-start(f32[128,256]{1,0:T(8,128)} %param.31) | copy-start | bytes 393220
  129.1 45.2 %copy-start.2 = (s32[640,256]{1,0:T(8,128)S(1)}, s32[640,256]{1,0:T(8,128)}, u32[]{:S(2)}) copy-start(s32[640,256]{1,0:T(8,128)} %copy-done.1) | copy-start | bytes 1966084
  165.2 9.2 %all-to-all-start.3 = ((bf16[4,160,256]{2,1,0:T(8,128)(2,1)}), bf16[4,160,256]{2,1,0:T(8,128)(2,1)S(1)}, u32[]{:S(2)}, u32[]{:S(2)}) async-start(bf16[4,160,256]{2,1,0:T(8,128)(2,1)} %reduce-scatter.3.cloned.1.call-done), calls=%async_computation.4 | async-start | bytes 655360 | tf_op jit(solution)/shard_map/all_to_all | solution.py:139
  168.8 27.8 %all-gather.7.cloned.1.call-start = ((), (), s32[]{:S(2)}) async-start(), calls=%async_computation.8 | async-start | bytes 1179648 | tf_op jit(solution)/shard_map/all_gather | solution.py:146
  175.4 7.5 %copy-start.19 = (bf16[640,896]{1,0:T(8,128)(2,1)S(1)}, bf16[640,896]{1,0:T(8,128)(2,1)}, u32[]{:S(2)}) copy-start(bf16[640,896]{1,0:T(8,128)(2,1)} %copy-done.18) | copy-start | bytes 3440644
  175.4 65.8 %reduce-scatter.5.cloned.1.call-start = ((), (), s32[]{:S(2)}) async-start(), calls=%async_computation.9 | async-start | bytes 655360 | tf_op jit(solution)/shard_map/reduce_scatter | solution.py:218
  175.5 7.4 %copy-start.16 = (bf16[4,160,2048]{2,1,0:T(8,128)(2,1)S(1)}, bf16[4,160,2048]{2,1,0:T(8,128)(2,1)}, u32[]{:S(2)}) copy-start(bf16[4,160,2048]{2,1,0:T(8,128)(2,1)} %all-gather.5.cloned.1.call-done) | copy-start | bytes 7864324
  182.9 4.9 %copy-start.4 = (bf16[80,8,8,256]{3,1,2,0:T(8,128)(2,1)S(1)}, bf16[80,8,8,256]{3,1,2,0:T(8,128)(2,1)}, u32[]{:S(2)}) copy-start(bf16[80,8,8,256]{3,1,2,0:T(8,128)(2,1)} %copy-done.3) | copy-start | bytes 7864324
  182.9 4.9 %copy-start.21 = (f32[640,896]{1,0:T(8,128)S(1)}, f32[640,896]{1,0:T(8,128)}, u32[]{:S(2)}) copy-start(f32[640,896]{1,0:T(8,128)} %fusion.3) | copy-start | bytes 6881284
  182.9 4.9 %copy-start.23 = (f32[640,896]{1,0:T(8,128)S(1)}, f32[640,896]{1,0:T(8,128)}, u32[]{:S(2)}) copy-start(f32[640,896]{1,0:T(8,128)} %fusion.7) | copy-start | bytes 6881284
  198.8 16.9 %copy-start.5 = (bf16[256,2048]{1,0:T(8,128)(2,1)S(1)}, bf16[256,2048]{1,0:T(8,128)(2,1)}, u32[]{:S(2)}) copy-start(bf16[256,2048]{1,0:T(8,128)(2,1)} %all-gather.7.cloned.1.call-done) | copy-start | bytes 3145732
Sparse Core Ops, SparseCore 0:
  25.2 50.7 all-gather.4
  129.3 35.8 reduce-scatter.2
  175.5 21.1 all-gather.6
  217.2 23.9 reduce-scatter.4
